TPU v7x, 32 devices: a whole 2x2x4 slice. The times are simulated.
32 devices in a mesh: sp: 8 (over z, x), tp: 4 (over y, core).
Axes of the slice: x: 2, y: 2, z: 4, core: 2. Of those that a mesh axis runs over, the one named last changes fastest.
Arguments:
- pool_input: bfloat16 [4096, 512], P('sp', 'tp'), may hold values from -6 to 6
- documents: int32 [4096], P('sp'), may hold values from 0 to 1, never falling along the last dimension, each value on 1 to 3072 neighbouring positions
- group_weight: bfloat16 [4, 128, 128], P('tp'), may hold values from -0.5 to 0.5
- pool_scale: float32 [512], P('tp'), may hold values from 0.15 to 4.2, as said below
- pool_gain: float32 [512], P('tp'), may hold values from 0.1 to 1.9
- out_weight: bfloat16 [512, 2048], P('tp'), may hold values from -0.25 to 0.25
- residual: bfloat16 [4096, 2048], P(('sp', 'tp')), may hold values from -6 to 6
- routing: int32 [4096, 2], P(('sp', 'tp')), may hold values from 0 to 7, all different within a row; in each aligned block of 128 rows (0 to 127, 128 to 255, ...) at most 48 rows name the same one
- route_weights: float32 [4096, 2], P(('sp', 'tp')), may hold values from 0.2 to 0.9
- ffn_gain: float32 [2048], replicated, may hold values from 0.1 to 1.9
- expert_gate: bfloat16 [8, 2048, 3584], P('sp', None, 'tp'), may hold values from -0.125 to 0.125
- expert_up: bfloat16 [8, 2048, 3584], P('sp', None, 'tp'), may hold values from -0.125 to 0.125
- expert_down: bfloat16 [8, 3584, 2048], P('sp', 'tp'), may hold values from -0.09375 to 0.09375
Outputs:
- mixed: bfloat16 [4096, 2048], P(('sp', 'tp'))
Inputs may be any that keep to these rules, and one draw needn't show every extreme that they name: `documents`: document numbers never fall along the sequence. `routing`: the two entries of a row differ. Among the rows of one device (128 rows in sp+tp order), no expert is named more than 48 times, a bound that some block reaches. `pool_scale`: Positive.
All inputs are finite; a program needn't handle non-finite values.
Results may differ from a plain program's by a relative error of at most 0.013.
Values may be sent and summed in bfloat16 or wider, within the bound.
A program may use at most 128 MiB of HBM per device.

v0:
```python
import functools

import jax
import jax.numpy as jnp
from jax import lax
from jax.experimental import pallas as pl
from jax.experimental.pallas import tpu as pltpu
from jax.sharding import PartitionSpec as P

epsilon = 1e-06


def xor_index(value, other, size):
    result, bit = 0, 1
    while bit < size:
        result = result + ((value // bit + other // bit) % 2) * bit
        bit *= 2
    return result


def offset_of(step, size):
    return step


def order_of(turn, size):
    return ((turn + size // 2 - 2) % (size - 1) + 1) * ((turn + size - 1) // size)


def remote(src, dst, sems, target):
    return pltpu.make_async_remote_copy(
        src_ref=src,
        dst_ref=dst,
        send_sem=sems[0],
        recv_sem=sems[1],
        device_id=target,
        device_id_type=pl.DeviceIdType.MESH,
    )


def turned(row, tokens):
    wide = jnp.broadcast_to(row, (tokens, row.shape[1]))
    return wide, wide.T


def moe_kernel(
    size,
    cap,
    pool,
    docs,
    group_weight,
    pool_scale,
    pool_gain,
    out_weight,
    residual,
    routing,
    route_weights,
    ffn_gain,
    gate_hbm,
    up_hbm,
    down_hbm,
    out,
    gate,
    up,
    down,
    sending,
    rows,
    part,
    from_core,
    from_y,
    back,
    acc,
    normed,
    slot_rows,
    slot_cols,
    weights,
    halo,
    halo_docs,
    gained,
    energy,
    far_gained,
    far_energy,
    wall,
    weight_sem,
    self_sem,
    d_s,
    d_r,
    y_s,
    y_r,
    c_s,
    c_r,
    p_s,
    p_r,
    q_s,
    q_r,
    t_s,
    t_r,
    halo_s,
    halo_r,
    wall_s,
    wall_r,
    gained_s,
    gained_r,
    energy_s,
    energy_r,
):
    me = lax.axis_index("sp")
    tp = lax.axis_index("tp")
    core, line = tp % 2, tp // 2
    place = core * 2 + line
    core_peer = {"tp": tp + 1 - 2 * core}
    line_peer = {"tp": (tp + 2) % 4}
    capp, width = sending.shape[1], sending.shape[2]
    tokens = residual.shape[0]

    loads = [
        pltpu.make_async_copy(src, dst, weight_sem.at[i])
        for i, (src, dst) in enumerate(((gate_hbm, gate), (up_hbm, up), (down_hbm, down)))
    ]
    for load in loads:
        load.start()

    row_ids = lax.broadcasted_iota(jnp.int32, (tokens, tokens), 0)
    col_ids = lax.broadcasted_iota(jnp.int32, (tokens, tokens), 1)

    def rank_slots():
        first_row, first_col = turned(routing[0:1, :].astype(jnp.float32), tokens)
        second_row, second_col = turned(routing[1:2, :].astype(jnp.float32), tokens)
        before, after = col_ids < row_ids, row_ids < col_ids

        def count(mask, axis):
            return jnp.sum(jnp.where(mask, 1.0, 0.0), axis=axis, keepdims=True)

        same_first, same_second = first_col == first_row, second_col == second_row
        slot_rows[0:1, :] = first_row[0:1, :] * cap + count(same_first & after, 0)
        slot_rows[1:2, :] = (
            second_row[0:1, :] * cap
            + count(first_col == second_row, 0)
            + count(same_second & after, 0)
        )
        slot_cols[0] = first_col * cap + count(same_first & before, 1)
        slot_cols[1] = (
            second_col * cap + count(second_col == first_row, 1) + count(same_second & before, 1)
        )
        weights[0] = turned(route_weights[0:1, :], tokens)[1]
        weights[1] = turned(route_weights[1:2, :], tokens)[1]

    def prefix():
        total = docs.shape[1]
        near = tp + 2 - 4 * line
        behind = [
            remote(
                pool.at[pl.ds(total - tokens, tokens)],
                halo,
                (halo_s.at[0], halo_r.at[0]),
                {"sp": (me + 1) % size},
            ),
            remote(
                docs.at[:, pl.ds(total - tokens, tokens)],
                halo_docs,
                (halo_s.at[1], halo_r.at[1]),
                {"sp": (me + 1) % size},
            ),
        ]

        @pl.when(me < size - 1)
        def _():
            for copy in behind:
                copy.start()

        to_line = remote(out_weight, wall.at[tp], (wall_s.at[0], wall_r.at[0]), line_peer)
        to_core = remote(out_weight, wall.at[tp], (wall_s.at[1], wall_r.at[1]), core_peer)
        relayed = remote(wall.at[near], wall.at[near], (wall_s.at[2], wall_r.at[2]), core_peer)
        to_line.start()
        to_core.start()

        @pl.when(me == 0)
        def _():
            halo[...] = jnp.zeros_like(halo)
            halo_docs[...] = jnp.full_like(halo_docs, -1)

        @pl.when(me > 0)
        def _():
            for copy in behind:
                copy.wait_recv()

        reach = 2 * (1 + core) * (1 + 3 * line)
        for index in range(total // tokens):
            here = pl.ds(index * tokens, tokens)
            before = pl.ds((index - 1) * tokens, tokens)
            own = pool[here, :]
            earlier = pool[before, :] if index else halo[...]
            doc_row, doc_col = turned(docs[:, here].astype(jnp.float32), tokens)
            old_row = (docs[:, before] if index else halo_docs[...]).astype(jnp.float32)
            inside = (doc_row == doc_col) & (col_ids <= row_ids) & (col_ids > row_ids - reach)
            outside = (old_row == doc_col) & (col_ids - tokens > row_ids - reach)
            inside = jnp.where(inside, 1.0, 0.0)
            outside = jnp.where(outside, 1.0, 0.0)
            counted = jnp.sum(inside + outside, axis=1, keepdims=True)
            running = jnp.dot(
                inside.astype(jnp.bfloat16), own, preferred_element_type=jnp.float32
            ) + jnp.dot(outside.astype(jnp.bfloat16), earlier, preferred_element_type=jnp.float32)
            difference = (running / counted - own.astype(jnp.float32)).astype(jnp.bfloat16)
            scaled = (
                jnp.dot(difference, group_weight[0], preferred_element_type=jnp.float32)
                * pool_scale[...]
            )
            gained[index] = (scaled * pool_gain[...]).astype(jnp.bfloat16)
            squares = jnp.sum((scaled * scaled).T, axis=0, keepdims=True)
            energy[index] = jnp.broadcast_to(squares, energy.shape[1:])

        def trade(away):
            to = (tp + away) % 4
            return (
                remote(
                    gained.at[to],
                    far_gained.at[away],
                    (gained_s.at[away], gained_r.at[away]),
                    {"tp": to},
                ),
                remote(
                    energy.at[to],
                    far_energy.at[away],
                    (energy_s.at[away], energy_r.at[away]),
                    {"tp": to},
                ),
            )

        for away in range(1, 4):
            for copy in trade(away):
                copy.start()
        acc[...] = jnp.dot(gained[tp], out_weight[...], preferred_element_type=jnp.float32)
        squared = energy[tp]
        for away in range(1, 4):
            for copy in trade(away):
                copy.wait_recv()
            squared = squared + far_energy[away]
        to_line.wait_recv()
        relayed.start()
        to_core.wait_recv()

        def project(source):
            away = (tp + 4 - source) % 4
            acc[...] += jnp.dot(
                far_gained[away], wall[source], preferred_element_type=jnp.float32
            )

        project(tp + 1 - 2 * core)
        project(near)
        relayed.wait_recv()
        project(near + 1 - 2 * core)
        energy_col = turned(squared[0:1, :], tokens)[1][:, 0:1]
        scale = lax.rsqrt(energy_col / (4 * pool.shape[1]) + epsilon)
        middle = (residual[...].astype(jnp.float32) + acc[...] * scale).astype(jnp.bfloat16)
        middle = middle.astype(jnp.float32)
        acc[...] = middle
        inverse = lax.rsqrt(jnp.mean(middle * middle, axis=1, keepdims=True) + epsilon)
        normed[...] = (middle * inverse * ffn_gain[...]).astype(jnp.bfloat16)

        @pl.when(me < size - 1)
        def _():
            for copy in behind:
                copy.wait_send()

        for copy in (to_line, to_core, relayed):
            copy.wait_send()
        for away in range(1, 4):
            for copy in trade(away):
                copy.wait_send()

    barrier = pltpu.get_barrier_semaphore()

    def greet(step, carry):
        peer = xor_index(me, offset_of(step, size), size)
        pl.semaphore_signal(
            barrier, inc=1, device_id={"sp": peer}, device_id_type=pl.DeviceIdType.MESH
        )
        return carry

    lax.fori_loop(1, size, greet, 0)
    for away in range(1, 4):
        pl.semaphore_signal(
            barrier,
            inc=1,
            device_id={"tp": (tp + away) % 4},
            device_id_type=pl.DeviceIdType.MESH,
        )
    rank_slots()
    pl.semaphore_wait(barrier, size + 2)
    prefix()

    def peer_of(step):
        return xor_index(me, offset_of(step, size), size)

    def dispatch(step):
        return remote(
            sending.at[step], rows.at[step, place], (d_s.at[step], d_r.at[step]), {"sp": peer_of(step)}
        )

    def across_line(step):
        return remote(
            rows.at[step, place], rows.at[step, place], (y_s.at[step], y_r.at[step]), line_peer
        )

    def across_core(step):
        block = rows.at[step, pl.ds(2 * core, 2)]
        return remote(block, block, (c_s.at[step], c_r.at[step]), core_peer)

    def core_sum(step):
        return remote(
            part.at[step, pl.ds(2 * (1 - core), 2)],
            from_core.at[step],
            (p_s.at[step], p_r.at[step]),
            core_peer,
        )

    def line_sum(step):
        return remote(
            part.at[step, 2 * core + 1 - line],
            from_y.at[step],
            (q_s.at[step], q_r.at[step]),
            line_peer,
        )

    def give_back(step):
        return remote(
            part.at[step, place], back.at[step], (t_s.at[step], t_r.at[step]), {"sp": peer_of(step)}
        )

    def filled(step):
        first = peer_of(step) * cap
        position = lax.broadcasted_iota(jnp.int32, (capp, tokens), 0)
        wanted = jnp.where(position < cap, position + first, -1).astype(jnp.float32)
        match = (wanted == slot_rows[0:1, :]) | (wanted == slot_rows[1:2, :])
        return jnp.dot(
            match.astype(jnp.float32).astype(jnp.bfloat16),
            normed[...],
            preferred_element_type=jnp.float32,
        ).astype(jnp.bfloat16)

    def send_rows(step, carry):
        sending[step] = filled(step)
        dispatch(step).start()
        return carry

    sending[0] = filled(0)
    own = pltpu.make_async_copy(sending.at[0], rows.at[0, place], self_sem.at[0])
    own.start()
    lax.fori_loop(1, size, send_rows, 0)
    own.wait()
    across_line(0).start()
    for load in loads:
        load.wait()

    def expert(step):
        block = rows[step]
        if capp % 16:
            block = block.astype(jnp.float32).reshape(4 * capp, width).astype(jnp.bfloat16)
        else:
            block = block.reshape(4 * capp, width)
        gate_sum = jnp.dot(block, gate[...], preferred_element_type=jnp.float32)
        up_sum = jnp.dot(block, up[...], preferred_element_type=jnp.float32)
        hidden = (gate_sum / (1.0 + jnp.exp(-gate_sum)) * up_sum).astype(jnp.bfloat16)
        result = jnp.dot(hidden, down[...], preferred_element_type=jnp.float32)
        part[step] = result.reshape(4, capp, width).astype(jnp.bfloat16)

    half = size // 2

    def arrive(step):
        dispatch(step).wait_recv()
        across_line(step).start()

    def share(step):
        across_line(step).wait_recv()
        across_core(step).start()

    def multiply(step):
        across_core(step).wait_recv()
        expert(step)
        core_sum(step).start()

    def reduce_core(step):
        core_sum(step).wait_recv()
        other = 2 * core + 1 - line
        total = part[step, other].astype(jnp.float32) + from_core[step, 1 - line].astype(
            jnp.float32
        )
        part[step, other] = total.astype(jnp.bfloat16)
        line_sum(step).start()

    def reduce_line(step):
        line_sum(step).wait_recv()
        total = (
            part[step, place].astype(jnp.float32)
            + from_core[step, line].astype(jnp.float32)
            + from_y[step].astype(jnp.float32)
        )
        part[step, place] = total.astype(jnp.bfloat16)

        @pl.when(step >= 1)
        def _():
            give_back(step).start()

    def early(step, carry):
        arrive(step)
        return carry

    def body(turn, carry):
        multiply(order_of(turn, size))

        @pl.when(turn >= 1)
        def _():
            reduce_line(order_of(turn - 1, size))

        @pl.when(turn + 1 < size)
        def _():
            share(order_of(turn + 1, size))

        reduce_core(order_of(turn, size))

        @pl.when((turn + 2 < size) & (order_of(turn + 2, size) >= half))
        def _():
            arrive(order_of(turn + 2, size))

        return carry

    lax.fori_loop(1, half, early, 0)
    share(0)
    multiply(0)
    arrive(half)
    reduce_core(0)
    arrive(half + 1)
    share(half)
    lax.fori_loop(1, size, body, 0)
    reduce_line(half - 1)

    def returned(step, carry):
        give_back(step).wait_recv()
        return carry

    back[0] = part[0, place]
    position = lax.broadcasted_iota(jnp.int32, (tokens, size * capp), 1)
    block, offset = position // capp, position % capp
    expert_of = xor_index(block, me, size)
    wanted = jnp.where(offset < cap, expert_of * cap + offset, -1).astype(jnp.float32)
    chosen = jnp.where(wanted == slot_cols[0, :, 0:1], weights[0, :, 0:1], 0.0) + jnp.where(
        wanted == slot_cols[1, :, 0:1], weights[1, :, 0:1], 0.0
    )
    high = chosen.astype(jnp.bfloat16)
    low = (chosen - high.astype(jnp.float32)).astype(jnp.bfloat16)
    lax.fori_loop(1, size, returned, 0)
    values = back[...]
    if capp % 16:
        values = values.astype(jnp.float32).reshape(size * capp, width).astype(jnp.bfloat16)
    else:
        values = values.reshape(size * capp, width)
    acc[...] += jnp.dot(high, values, preferred_element_type=jnp.float32) + jnp.dot(
        low, values, preferred_element_type=jnp.float32
    )
    out[...] = acc[...].astype(jnp.bfloat16)

    def finish(step, carry):
        @pl.when(step >= 1)
        def _():
            dispatch(step).wait_send()
            give_back(step).wait_send()

        across_line(step).wait_send()
        across_core(step).wait_send()
        core_sum(step).wait_send()
        line_sum(step).wait_send()
        return carry

    lax.fori_loop(0, size, finish, 0)


def on_device(
    pool_input,
    documents,
    group_weight,
    pool_scale,
    pool_gain,
    out_weight,
    residual,
    routing,
    route_weights,
    ffn_gain,
    expert_gate,
    expert_up,
    expert_down,
):
    size = lax.axis_size("sp")
    tokens, width = residual.shape
    channels = pool_input.shape[1]
    gate, up, down = expert_gate[0], expert_up[0], expert_down[0]
    capacity = (3 * tokens + size - 1) // size
    padded = (capacity + 7) // 8 * 8
    vmem = pl.BlockSpec(memory_space=pltpu.VMEM)
    hbm = pl.BlockSpec(memory_space=pl.ANY)
    block = (padded, width)
    return pl.pallas_call(
        functools.partial(moe_kernel, size, capacity),
        out_shape=jax.ShapeDtypeStruct((tokens, width), jnp.bfloat16),
        in_specs=[vmem] * 10 + [hbm] * 3,
        out_specs=vmem,
        scratch_shapes=[
            pltpu.VMEM(gate.shape, jnp.bfloat16),
            pltpu.VMEM(up.shape, jnp.bfloat16),
            pltpu.VMEM(down.shape, jnp.bfloat16),
            pltpu.VMEM((size,) + block, jnp.bfloat16),
            pltpu.VMEM((size, 4) + block, jnp.bfloat16),
            pltpu.VMEM((size, 4) + block, jnp.bfloat16),
            pltpu.VMEM((size, 2) + block, jnp.bfloat16),
            pltpu.VMEM((size,) + block, jnp.bfloat16),
            pltpu.VMEM((size,) + block, jnp.bfloat16),
            pltpu.VMEM((tokens, width), jnp.float32),
            pltpu.VMEM((tokens, width), jnp.bfloat16),
            pltpu.VMEM((2, tokens), jnp.float32),
            pltpu.VMEM((2, tokens, tokens), jnp.float32),
            pltpu.VMEM((2, tokens, tokens), jnp.float32),
            pltpu.VMEM((tokens, channels), jnp.bfloat16),
            pltpu.VMEM((1, tokens), jnp.int32),
            pltpu.VMEM((4, tokens, channels), jnp.bfloat16),
            pltpu.VMEM((4, 8, tokens), jnp.float32),
            pltpu.VMEM((4, tokens, channels), jnp.bfloat16),
            pltpu.VMEM((4, 8, tokens), jnp.float32),
            pltpu.VMEM((4, channels, width), jnp.bfloat16),
            pltpu.SemaphoreType.DMA((3,)),
            pltpu.SemaphoreType.DMA((1,)),
        ]
        + [pltpu.SemaphoreType.DMA((size,))] * 12
        + [pltpu.SemaphoreType.DMA((2,))] * 2
        + [pltpu.SemaphoreType.DMA((3,))] * 2
        + [pltpu.SemaphoreType.DMA((4,))] * 4,
        compiler_params=pltpu.CompilerParams(
            collective_id=0, has_side_effects=True, vmem_limit_bytes=62 * 1024 * 1024
        ),
    )(
        pool_input,
        documents.reshape(1, -1),
        group_weight,
        pool_scale.reshape(1, -1),
        pool_gain.reshape(1, -1),
        out_weight,
        residual,
        routing.T,
        route_weights.T,
        ffn_gain.reshape(1, -1),
        gate,
        up,
        down,
    )


def solution(mesh):
    return jax.shard_map(
        on_device,
        mesh=mesh,
        in_specs=(
            P("sp", "tp"),
            P("sp"),
            P("tp", None, None),
            P("tp"),
            P("tp"),
            P("tp", None),
            P(("sp", "tp"), None),
            P(("sp", "tp"), None),
            P(("sp", "tp"), None),
            P(),
            P("sp", None, "tp"),
            P("sp", None, "tp"),
            P("sp", "tp", None),
        ),
        out_specs=P(("sp", "tp"), None),
        check_vma=False,
    )
```

profile of v0, /device:TPU:0, one launch (start us, length us, event | category | flops | bytes accessed | tf_op | source)
XLA Modules:
  0.0 116.9 jit_solution(9575402599415228287)
XLA Ops:
  0.0 115.0 %shard_map.127 = bf16[128,2048]{1,0:T(8,128)(2,1)} custom-call(bf16[512,128]{1,0:T(8,128)(2,1)} %pool.1, s32[1,512]{1,0:T(1,128)} %bitcast.13, bf16[1,128,128]{2,1,0:T(8,128)(2,1)} %group_weight.1, f32[1,128]{1,0:T(1,128)} %bitcast.16, f32[1,128]{1,0:T(1,128)} %bitcast.17, bf16[128,2048]{1,0:T(8,128)(2,1)} %out_weight.1, bf16[128,2048]{1,0:T(8,128)(2,1)} %residual.1, ...), custom_call_target="tpu_custom_call" | custom-call | tf_op jit(solution)/shard_map/pallas_call | solution.py:500
  115.0 1.9 %copy.15 = bf16[128,2048]{1,0:T(8,128)(2,1)} copy(bf16[128,2048]{1,0:T(8,128)(2,1)} %shard_map.127) | data formatting | bytes 1048576
where the time goes:
time: 118 us; the launch traced here: 117 us
  Pallas kernels  115 us (97%)
  local copies, waits for them, and re-layouts  1.88 us (2%)
    pallas_call x1, Pallas kernels, on_device(): pl.pallas_call(functools.partial(moe_kernel, size, capacity), out_shape=j...  115 us

commit v1 on v0

--- a/solution.py
+++ b/solution.py
@@ -18,12 +18,22 @@
     return result
 
 
-def offset_of(step, size):
-    return step
+def far_of(index, size):
+    return size // 2 + index % 2 * (size // 4) + index // 2
 
 
 def order_of(turn, size):
-    return ((turn + size // 2 - 2) % (size - 1) + 1) * ((turn + size - 1) // size)
+    half = size // 2
+    late = turn // half
+    return (1 - late) * far_of(turn % half, size) + late * (size - 1 - turn)
+
+
+def sent_at(turn, me, size):
+    half = size // 2
+    far = turn // half
+    swap = (me // 2 + me // 4 + 1) % 2
+    step = (1 - far) * turn + far * (half + turn % half % 2 * (size // 4) + turn % half // 2)
+    return xor_index(step, far * swap * (size // 4), size)
 
 
 def remote(src, dst, sems, target):
@@ -62,6 +72,7 @@
     gate,
     up,
     down,
+    hidden,
     sending,
     rows,
     part,
@@ -167,24 +178,45 @@
             for copy in behind:
                 copy.start()
 
-        to_line = remote(out_weight, wall.at[tp], (wall_s.at[0], wall_r.at[0]), line_peer)
-        to_core = remote(out_weight, wall.at[tp], (wall_s.at[1], wall_r.at[1]), core_peer)
-        relayed = remote(wall.at[near], wall.at[near], (wall_s.at[2], wall_r.at[2]), core_peer)
-        to_line.start()
+        side = me % 2
+        piece = out_weight.shape[0] // 8
+
+        def strip(first, count):
+            return pl.ds(pl.multiple_of(first * piece, piece), count * piece)
+
+        def moved(src, place, index, target):
+            return remote(src, place, (wall_s.at[index], wall_r.at[index]), target)
+
+        def handed_on(rows_of, index, target):
+            block = wall.at[near, rows_of]
+            return moved(block, block, index, target)
+
+        mine = [strip(5 * side + i, 1) for i in range(3)]
+        middle_rows = strip(3, 2)
+        to_line = [
+            moved(out_weight.at[rows_of], wall.at[tp, rows_of], i, line_peer)
+            for i, rows_of in enumerate([*mine, middle_rows])
+        ]
+        to_side = [
+            handed_on(rows_of, 4 + i, {"sp": me + 1 - 2 * side}) for i, rows_of in enumerate(mine)
+        ]
+        from_side = [
+            handed_on(strip(5 * (1 - side) + i, 1), 4 + i, {"sp": me + 1 - 2 * side})
+            for i in range(3)
+        ]
+        to_core = moved(out_weight, wall.at[tp], 7, core_peer)
+        relayed = [
+            handed_on(rows_of, 8 + i, core_peer)
+            for i, rows_of in enumerate(
+                [strip(5 * side, 3), strip(5 * (1 - side), 3), middle_rows]
+            )
+        ]
+        for copy in to_line[:3]:
+            copy.start()
         to_core.start()
 
-        @pl.when(me == 0)
-        def _():
-            halo[...] = jnp.zeros_like(halo)
-            halo_docs[...] = jnp.full_like(halo_docs, -1)
-
-        @pl.when(me > 0)
-        def _():
-            for copy in behind:
-                copy.wait_recv()
-
         reach = 2 * (1 + core) * (1 + 3 * line)
-        for index in range(total // tokens):
+        def pooled(index):
             here = pl.ds(index * tokens, tokens)
             before = pl.ds((index - 1) * tokens, tokens)
             own = pool[here, :]
@@ -208,6 +240,21 @@
             squares = jnp.sum((scaled * scaled).T, axis=0, keepdims=True)
             energy[index] = jnp.broadcast_to(squares, energy.shape[1:])
 
+        for index in range(1, total // tokens):
+            pooled(index)
+
+        @pl.when(me == 0)
+        def _():
+            halo[...] = jnp.zeros_like(halo)
+            halo_docs[...] = jnp.full_like(halo_docs, -1)
+
+        @pl.when(me > 0)
+        def _():
+            for copy in behind:
+                copy.wait_recv()
+
+        pooled(0)
+
         def trade(away):
             to = (tp + away) % 4
             return (
@@ -228,15 +275,17 @@
         for away in range(1, 4):
             for copy in trade(away):
                 copy.start()
+        to_line[3].start()
         acc[...] = jnp.dot(gained[tp], out_weight[...], preferred_element_type=jnp.float32)
+        for arrived, onward in zip(to_line[:3], to_side):
+            arrived.wait_recv()
+            onward.start()
+        relayed[0].start()
         squared = energy[tp]
         for away in range(1, 4):
             for copy in trade(away):
                 copy.wait_recv()
             squared = squared + far_energy[away]
-        to_line.wait_recv()
-        relayed.start()
-        to_core.wait_recv()
 
         def project(source):
             away = (tp + 4 - source) % 4
@@ -244,9 +293,16 @@
                 far_gained[away], wall[source], preferred_element_type=jnp.float32
             )
 
+        to_core.wait_recv()
         project(tp + 1 - 2 * core)
+        to_line[3].wait_recv()
+        relayed[2].start()
+        for copy in from_side:
+            copy.wait_recv()
+        relayed[1].start()
         project(near)
-        relayed.wait_recv()
+        for copy in relayed:
+            copy.wait_recv()
         project(near + 1 - 2 * core)
         energy_col = turned(squared[0:1, :], tokens)[1][:, 0:1]
         scale = lax.rsqrt(energy_col / (4 * pool.shape[1]) + epsilon)
@@ -261,7 +317,7 @@
             for copy in behind:
                 copy.wait_send()
 
-        for copy in (to_line, to_core, relayed):
+        for copy in (*to_line, *to_side, to_core, *relayed):
             copy.wait_send()
         for away in range(1, 4):
             for copy in trade(away):
@@ -270,7 +326,7 @@
     barrier = pltpu.get_barrier_semaphore()
 
     def greet(step, carry):
-        peer = xor_index(me, offset_of(step, size), size)
+        peer = xor_index(me, step, size)
         pl.semaphore_signal(
             barrier, inc=1, device_id={"sp": peer}, device_id_type=pl.DeviceIdType.MESH
         )
@@ -289,7 +345,7 @@
     prefix()
 
     def peer_of(step):
-        return xor_index(me, offset_of(step, size), size)
+        return xor_index(me, step, size)
 
     def dispatch(step):
         return remote(
@@ -337,7 +393,8 @@
             preferred_element_type=jnp.float32,
         ).astype(jnp.bfloat16)
 
-    def send_rows(step, carry):
+    def send_rows(turn, carry):
+        step = sent_at(turn, me, size)
         sending[step] = filled(step)
         dispatch(step).start()
         return carry
@@ -351,7 +408,7 @@
     for load in loads:
         load.wait()
 
-    def expert(step):
+    def gate_up(step):
         block = rows[step]
         if capp % 16:
             block = block.astype(jnp.float32).reshape(4 * capp, width).astype(jnp.bfloat16)
@@ -359,8 +416,10 @@
             block = block.reshape(4 * capp, width)
         gate_sum = jnp.dot(block, gate[...], preferred_element_type=jnp.float32)
         up_sum = jnp.dot(block, up[...], preferred_element_type=jnp.float32)
-        hidden = (gate_sum / (1.0 + jnp.exp(-gate_sum)) * up_sum).astype(jnp.bfloat16)
-        result = jnp.dot(hidden, down[...], preferred_element_type=jnp.float32)
+        hidden[...] = (gate_sum / (1.0 + jnp.exp(-gate_sum)) * up_sum).astype(jnp.bfloat16)
+
+    def downward(step):
+        result = jnp.dot(hidden[...], down[...], preferred_element_type=jnp.float32)
         part[step] = result.reshape(4, capp, width).astype(jnp.bfloat16)
 
     half = size // 2
@@ -372,11 +431,6 @@
     def share(step):
         across_line(step).wait_recv()
         across_core(step).start()
-
-    def multiply(step):
-        across_core(step).wait_recv()
-        expert(step)
-        core_sum(step).start()
 
     def reduce_core(step):
         core_sum(step).wait_recv()
@@ -400,38 +454,60 @@
         def _():
             give_back(step).start()
 
+    def body(turn, carry):
+        step = order_of(turn, size)
+        across_core(step).wait_recv()
+        gate_up(step)
+
+        @pl.when(turn >= half + 1)
+        def _():
+            reduce_core(order_of(turn - 1, size))
+
+        downward(step)
+        core_sum(step).start()
+
+        @pl.when(turn + 2 < half)
+        def _():
+            arrive(far_of(turn + 2, size))
+
+        @pl.when(turn < half)
+        def _():
+            reduce_core(step)
+
+        @pl.when(turn + 1 < half)
+        def _():
+            share(far_of(turn + 1, size))
+
+        @pl.when((turn >= 1) & (turn < half))
+        def _():
+            reduce_line(order_of(turn - 1, size))
+
+        @pl.when(turn >= half + 1)
+        def _():
+            reduce_line(order_of(turn - 2, size))
+
+        return carry
+
+    def near(step, carry):
+        share(step)
+        return carry
+
+    arrive(1)
+    share(0)
+
     def early(step, carry):
         arrive(step)
         return carry
 
-    def body(turn, carry):
-        multiply(order_of(turn, size))
-
-        @pl.when(turn >= 1)
-        def _():
-            reduce_line(order_of(turn - 1, size))
-
-        @pl.when(turn + 1 < size)
-        def _():
-            share(order_of(turn + 1, size))
-
-        reduce_core(order_of(turn, size))
-
-        @pl.when((turn + 2 < size) & (order_of(turn + 2, size) >= half))
-        def _():
-            arrive(order_of(turn + 2, size))
-
-        return carry
-
-    lax.fori_loop(1, half, early, 0)
-    share(0)
-    multiply(0)
-    arrive(half)
+    lax.fori_loop(2, half, early, 0)
+    arrive(far_of(0, size))
+    lax.fori_loop(1, half, near, 0)
+    arrive(far_of(1, size))
+    share(far_of(0, size))
+    lax.fori_loop(0, size, body, 0)
     reduce_core(0)
-    arrive(half + 1)
-    share(half)
-    lax.fori_loop(1, size, body, 0)
-    reduce_line(half - 1)
+    reduce_line(1)
+    reduce_line(0)
 
     def returned(step, carry):
         give_back(step).wait_recv()
@@ -506,6 +582,7 @@
             pltpu.VMEM(gate.shape, jnp.bfloat16),
             pltpu.VMEM(up.shape, jnp.bfloat16),
             pltpu.VMEM(down.shape, jnp.bfloat16),
+            pltpu.VMEM((4 * padded, down.shape[0]), jnp.bfloat16),
             pltpu.VMEM((size,) + block, jnp.bfloat16),
             pltpu.VMEM((size, 4) + block, jnp.bfloat16),
             pltpu.VMEM((size, 4) + block, jnp.bfloat16),
@@ -529,7 +606,7 @@
         ]
         + [pltpu.SemaphoreType.DMA((size,))] * 12
         + [pltpu.SemaphoreType.DMA((2,))] * 2
-        + [pltpu.SemaphoreType.DMA((3,))] * 2
+        + [pltpu.SemaphoreType.DMA((11,))] * 2
         + [pltpu.SemaphoreType.DMA((4,))] * 4,
         compiler_params=pltpu.CompilerParams(
             collective_id=0, has_side_effects=True, vmem_limit_bytes=62 * 1024 * 1024

time: 118 us -> 107 us (0.907)
  Pallas kernels: 115 us -> 105 us
    pallas_call x1, Pallas kernels: 115 us -> 105 us  [on_device(): pl.pallas_call(functools.partial(moe_kernel, size, capacity), out_shape=j...]
where the time goes in v1:
time: 107 us
  Pallas kernels  105 us (98%)
  local copies, waits for them, and re-layouts  1.88 us (2%)
    pallas_call x1, Pallas kernels, on_device(): pl.pallas_call(functools.partial(moe_kernel, size, capacity), out_shape=j...  105 us

profile of v1, /device:TPU:0, one launch (start us, length us, event | category | flops | bytes accessed | tf_op | source)
XLA Modules:
  0.0 106.9 jit_solution(13113184629809166001)
XLA Ops:
  0.0 105.0 %shard_map.127 = bf16[128,2048]{1,0:T(8,128)(2,1)} custom-call(bf16[512,128]{1,0:T(8,128)(2,1)} %pool.1, s32[1,512]{1,0:T(1,128)} %bitcast.13, bf16[1,128,128]{2,1,0:T(8,128)(2,1)} %group_weight.1, f32[1,128]{1,0:T(1,128)} %bitcast.16, f32[1,128]{1,0:T(1,128)} %bitcast.17, bf16[128,2048]{1,0:T(8,128)(2,1)} %out_weight.1, bf16[128,2048]{1,0:T(8,128)(2,1)} %residual.1, ...), custom_call_target="tpu_custom_call" | custom-call | tf_op jit(solution)/shard_map/pallas_call | solution.py:576
  105.0 1.9 %copy.15 = bf16[128,2048]{1,0:T(8,128)(2,1)} copy(bf16[128,2048]{1,0:T(8,128)(2,1)} %shard_map.127) | data formatting | bytes 1048576

commit v2 on v1

--- a/solution.py
+++ b/solution.py
@@ -24,16 +24,16 @@
 
 def order_of(turn, size):
     half = size // 2
-    late = turn // half
-    return (1 - late) * far_of(turn % half, size) + late * (size - 1 - turn)
-
-
-def sent_at(turn, me, size):
-    half = size // 2
-    far = turn // half
-    swap = (me // 2 + me // 4 + 1) % 2
-    step = (1 - far) * turn + far * (half + turn % half % 2 * (size // 4) + turn % half // 2)
-    return xor_index(step, far * swap * (size // 4), size)
+    early = (size - turn) // (half + 2)
+    last = turn // half * ((size - 1 - turn) // (half - 1))
+    far = early + last
+    return far * far_of((turn - last) % half, size) + (1 - far) * (size - 1 - turn - (size - turn) // (half + 1))
+
+
+def sent_at(turn, size):
+    odd, last = turn % 2, turn // (size - 2)
+    far = odd + last
+    return far * far_of(turn // 2, size) + (1 - far) * (turn // 2 + 1)
 
 
 def remote(src, dst, sems, target):
@@ -92,7 +92,6 @@
     far_energy,
     wall,
     weight_sem,
-    self_sem,
     d_s,
     d_r,
     y_s,
@@ -394,17 +393,14 @@
         ).astype(jnp.bfloat16)
 
     def send_rows(turn, carry):
-        step = sent_at(turn, me, size)
+        step = sent_at(turn, size)
         sending[step] = filled(step)
         dispatch(step).start()
         return carry
 
-    sending[0] = filled(0)
-    own = pltpu.make_async_copy(sending.at[0], rows.at[0, place], self_sem.at[0])
-    own.start()
-    lax.fori_loop(1, size, send_rows, 0)
-    own.wait()
+    rows[0, place] = filled(0)
     across_line(0).start()
+    lax.fori_loop(0, size - 1, send_rows, 0)
     for load in loads:
         load.wait()
 
@@ -456,53 +452,53 @@
 
     def body(turn, carry):
         step = order_of(turn, size)
+
+        @pl.when(turn + 1 < half)
+        def _():
+            arrive(far_of(turn + 1, size))
+
         across_core(step).wait_recv()
         gate_up(step)
 
-        @pl.when(turn >= half + 1)
+        @pl.when(turn == half - 1)
+        def _():
+            share(far_of(turn, size))
+
+        @pl.when((turn >= half) & (turn != half + 1))
         def _():
             reduce_core(order_of(turn - 1, size))
+
+        @pl.when(turn >= half)
+        def _():
+            reduce_line(order_of(turn - 2, size))
 
         downward(step)
         core_sum(step).start()
 
+        @pl.when((turn + 1 < half) | (turn == half))
+        def _():
+            reduce_core(step)
+
+        @pl.when(turn + 3 < half)
+        def _():
+            arrive(turn + 3)
+
+        @pl.when((turn >= 1) & (turn + 1 < half))
+        def _():
+            reduce_line(order_of(turn - 1, size))
+            share(turn + 1)
+
         @pl.when(turn + 2 < half)
         def _():
-            arrive(far_of(turn + 2, size))
-
-        @pl.when(turn < half)
-        def _():
-            reduce_core(step)
-
-        @pl.when(turn + 1 < half)
-        def _():
             share(far_of(turn + 1, size))
 
-        @pl.when((turn >= 1) & (turn < half))
-        def _():
-            reduce_line(order_of(turn - 1, size))
-
-        @pl.when(turn >= half + 1)
-        def _():
-            reduce_line(order_of(turn - 2, size))
-
         return carry
 
-    def near(step, carry):
-        share(step)
-        return carry
-
     arrive(1)
+    arrive(far_of(0, size))
     share(0)
-
-    def early(step, carry):
-        arrive(step)
-        return carry
-
-    lax.fori_loop(2, half, early, 0)
-    arrive(far_of(0, size))
-    lax.fori_loop(1, half, near, 0)
-    arrive(far_of(1, size))
+    share(1)
+    arrive(2)
     share(far_of(0, size))
     lax.fori_loop(0, size, body, 0)
     reduce_core(0)
@@ -602,7 +598,6 @@
             pltpu.VMEM((4, 8, tokens), jnp.float32),
             pltpu.VMEM((4, channels, width), jnp.bfloat16),
             pltpu.SemaphoreType.DMA((3,)),
-            pltpu.SemaphoreType.DMA((1,)),
         ]
         + [pltpu.SemaphoreType.DMA((size,))] * 12
         + [pltpu.SemaphoreType.DMA((2,))] * 2

time: 107 us -> 101 us (0.944)
  Pallas kernels: 105 us -> 98.5 us
    pallas_call x1, Pallas kernels: 105 us -> 98.5 us  [on_device(): pl.pallas_call(functools.partial(moe_kernel, size, capacity), out_shape=j...]
where the time goes in v2:
time: 101 us; the launch traced here: 100 us
  Pallas kernels  98.5 us (98%)
  local copies, waits for them, and re-layouts  1.88 us (2%)
    pallas_call x1, Pallas kernels, on_device(): pl.pallas_call(functools.partial(moe_kernel, size, capacity), out_shape=j...  98.5 us

profile of v2, /device:TPU:0, one launch (start us, length us, event | category | flops | bytes accessed | tf_op | source)
XLA Modules:
  0.0 100.4 jit_solution(7269712626544491773)
XLA Ops:
  0.0 98.5 %shard_map.127 = bf16[128,2048]{1,0:T(8,128)(2,1)} custom-call(bf16[512,128]{1,0:T(8,128)(2,1)} %pool.1, s32[1,512]{1,0:T(1,128)} %bitcast.13, bf16[1,128,128]{2,1,0:T(8,128)(2,1)} %group_weight.1, f32[1,128]{1,0:T(1,128)} %bitcast.16, f32[1,128]{1,0:T(1,128)} %bitcast.17, bf16[128,2048]{1,0:T(8,128)(2,1)} %out_weight.1, bf16[128,2048]{1,0:T(8,128)(2,1)} %residual.1, ...), custom_call_target="tpu_custom_call" | custom-call | tf_op jit(solution)/shard_map/pallas_call | solution.py:572
  98.5 1.9 %copy.15 = bf16[128,2048]{1,0:T(8,128)(2,1)} copy(bf16[128,2048]{1,0:T(8,128)(2,1)} %shard_map.127) | data formatting | bytes 1048576
